TPU v7x, 32 devices: a whole 2x2x4 slice. The times are simulated.
32 devices in a mesh: rep: 2 (over x), fs: 4 (over z), tp: 4 (over y, core).
Axes of the slice: x: 2, y: 2, z: 4, core: 2. Of those that a mesh axis runs over, the one named last changes fastest.
Arguments:
- tokens: bfloat16 [4096, 2048], P(('rep', 'fs', 'tp')), may hold values from -6 to 6
- norm_gain: float32 [2048], replicated, may hold values from 0.1 to 1.9
- gate_weight: float32 [2048, 5632], P('fs', 'tp'), may hold values from -0.125 to 0.125
- gate_scale: float32 [5632], P('tp'), may hold values from 0.5 to 2
- up_weight: float32 [2048, 5632], P('fs', 'tp'), may hold values from -0.125 to 0.125
- up_scale: float32 [5632], P('tp'), may hold values from 0.5 to 2
- down_weight: float32 [5632, 2048], P('tp', 'fs'), may hold values from -0.078125 to 0.078125
- down_scale: float32 [2048], P('fs'), may hold values from 0.5 to 2
Outputs:
- mixed: bfloat16 [4096, 2048], P(('rep', 'fs', 'tp'))
All inputs are finite; a program needn't handle non-finite values.
Results may differ from a plain program's by a relative error of at most 0.014.
Values may be sent and summed in bfloat16 or wider, within the bound.
A program may use at most 64 MiB of HBM per device.

v0:
```python
import jax
import jax.numpy as jnp
from jax import lax
from jax.sharding import PartitionSpec as P


def shards(
    tokens, norm_gain, gate_weight, gate_scale, up_weight, up_scale, down_weight, down_scale
):
    n_rep = lax.axis_size("rep")
    rep = lax.axis_index("rep")
    width = gate_weight.shape[1] // n_rep
    start = rep * width

    def part(array, axis):
        return lax.dynamic_slice_in_dim(array, start, width, axis)

    flat = tokens.astype(jnp.float32)
    mean_square = jnp.mean(flat * flat, axis=-1, keepdims=True)
    inverse = lax.rsqrt(mean_square + 1e-06)
    normed = (flat * inverse * norm_gain).astype(jnp.bfloat16)
    group = lax.all_gather(normed, ("rep", "tp"), axis=0, tiled=True)
    gate_low = part(gate_weight, 1).astype(jnp.bfloat16)
    up_low = part(up_weight, 1).astype(jnp.bfloat16)
    down_low = part(down_weight, 0).astype(jnp.bfloat16)
    gate = jnp.dot(
        group,
        lax.all_gather(gate_low, "fs", axis=0, tiled=True),
        preferred_element_type=jnp.float32,
    )
    up = jnp.dot(
        group, lax.all_gather(up_low, "fs", axis=0, tiled=True), preferred_element_type=jnp.float32
    )
    down_full = lax.all_gather(down_low, "fs", axis=1, tiled=True)
    gate = gate * part(gate_scale, 0)
    up = up * part(up_scale, 0)
    hidden = (jax.nn.silu(gate) * up).astype(jnp.bfloat16)
    scales = lax.all_gather(down_scale, "fs", axis=0, tiled=True)
    total = lax.psum_scatter(
        jnp.dot(hidden, down_full, preferred_element_type=jnp.float32).astype(jnp.bfloat16),
        ("rep", "tp"),
        scatter_dimension=0,
        tiled=True,
    ).astype(jnp.float32)
    return (total * scales).astype(jnp.bfloat16)


def solution(mesh):
    in_specs = (
        P(("rep", "fs", "tp"), None),
        P(),
        P("fs", "tp"),
        P("tp"),
        P("fs", "tp"),
        P("tp"),
        P("tp", "fs"),
        P("fs"),
    )
    out_specs = P(("rep", "fs", "tp"), None)
    return jax.shard_map(shards, mesh=mesh, in_specs=in_specs, out_specs=out_specs, check_vma=False)
```

profile of v0, /device:TPU:0, one launch (start us, length us, event | category | flops | bytes accessed | tf_op | source)
XLA Modules:
  0.0 308.1 jit_solution(6207909742359432319)
XLA Ops:
  6.5 0.0 copy-start
  6.5 0.0 copy-start.1
  6.5 0.0 copy-start.2
  6.5 0.0 all-gather.8.cloned.1.call-start
  6.6 1.8 copy-done
  8.4 1.2 dynamic-slice_convert_fusion.1
  9.6 0.0 all-gather.8.cloned.1.call-update
  9.6 0.0 all-gather.6.cloned.1.call-start
  9.7 1.2 fusion
  10.9 0.0 copy-done.1
  10.9 0.0 copy-done.2
  10.9 0.0 copy-start.4
  10.9 0.0 copy-start.5
  10.9 1.0 fusion.2
  11.9 0.0 all-gather.6.cloned.1.call-update
  11.9 0.0 all-gather.10.cloned.1.call-start
  12.0 2.7 dynamic-slice_convert_fusion
  14.7 0.0 all-gather.10.cloned.1.call-update
  14.8 0.0 all-gather.12.cloned.1.call-start
  14.8 2.3 dynamic-slice_convert_fusion.2
  17.1 0.0 all-gather.12.cloned.1.call-update
  17.2 0.0 reduce-scatter.2.cloned.1.call-start
  17.2 0.0 copy-done.4
  17.2 0.1 dynamic_slice.16
  17.3 0.0 copy-done.5
  17.3 0.1 dynamic_slice.18
  17.4 58.6 %all-gather.8.cloned.1.call-done = bf16[2048,704]{1,0:T(8,128)(2,1)} async-done(((bf16[512,704]{1,0:T(8,128)(2,1)}), bf16[2048,704]{1,0:T(8,128)(2,1)}) %all-gather.8.cloned.1.call-update) | async-done | bytes 2883600 | tf_op jit(solution)/shard_map/all_gather | solution.py:28
  75.9 37.1 %all-gather.6.cloned.1.call-done = bf16[1024,2048]{1,0:T(8,128)(2,1)} async-done(((bf16[128,2048]{1,0:T(8,128)(2,1)}), bf16[1024,2048]{1,0:T(8,128)(2,1)}) %all-gather.6.cloned.1.call-update) | async-done | bytes 4194320 | tf_op jit(solution)/shard_map/all_gather | solution.py:22
  113.1 7.9 %fusion.4 = f32[1024,704]{0,1:T(8,128)} fusion(bf16[1024,2048]{1,0:T(8,128)(2,1)} %all-gather.6.cloned.1.call-done, bf16[2048,704]{1,0:T(8,128)(2,1)} %all-gather.8.cloned.1.call-done), kind=kOutput, calls=%fused_computation.13 | convolution fusion | flops 2952790016 | bytes 9961472 | tf_op jit(solution)/shard_map/dot_general | solution.py:26
  121.0 57.1 %all-gather.10.cloned.1.call-done = bf16[2048,704]{1,0:T(8,128)(2,1)} async-done(((bf16[512,704]{1,0:T(8,128)(2,1)}), bf16[2048,704]{1,0:T(8,128)(2,1)}) %all-gather.10.cloned.1.call-update) | async-done | bytes 2883600 | tf_op jit(solution)/shard_map/all_gather | solution.py:32
  178.1 59.2 %all-gather.12.cloned.1.call-done = bf16[704,2048]{1,0:T(8,128)(2,1)} async-done(((bf16[704,512]{1,0:T(8,128)(2,1)}), bf16[704,2048]{1,0:T(8,128)(2,1)}) %all-gather.12.cloned.1.call-update) | async-done | bytes 2883600 | tf_op jit(solution)/shard_map/all_gather | solution.py:34
  237.3 12.3 %convolution_convert_fusion = bf16[1024,2048]{1,0:T(8,128)(2,1)} fusion(bf16[704,2048]{1,0:T(8,128)(2,1)} %all-gather.12.cloned.1.call-done, f32[1024,704]{0,1:T(8,128)} %fusion.4, bf16[1024,2048]{1,0:T(8,128)(2,1)} %all-gather.6.cloned.1.call-done, bf16[2048,704]{1,0:T(8,128)(2,1)} %all-gather.10.cloned.1.call-done, f32[704]{0:T(1024)S(1)} %dynamic_slice.18, ...), kind=kOutput, calls=%fused_computation | convolution fusion | flops 5913444352 | bytes 17044992 | tf_op jit(solution)/shard_map/dot_general | solution.py:40
  249.7 0.0 copy-start.3
  249.7 0.0 reduce-scatter.2.cloned.1.call-update
  249.7 0.7 copy-done.3
  250.3 11.9 %all-gather = f32[4,1,512]{2,1,0:T(1,128)S(1)} all-gather(f32[1,1,512]{2,1,0:T(1,128)S(1)} %bitcast.8), channel_id=1, replica_groups=mesh['rep'=2,'fs'=4,'tp'=4] {'fs'}, dimensions={0}, use_global_device_ids=true | all-gather | bytes 10240 | tf_op jit(solution)/shard_map/all_gather | solution.py:38
  262.3 37.4 %reduce-scatter.2.cloned.1.call-done = bf16[128,2048]{1,0:T(8,128)(2,1)} async-done(((bf16[1024,2048]{1,0:T(8,128)(2,1)}), bf16[128,2048]{1,0:T(8,128)(2,1)}) %reduce-scatter.2.cloned.1.call-update) | async-done | bytes 524304 | tf_op jit(solution)/shard_map/reduce_scatter | solution.py:39
  299.7 1.9 multiply_convert_fusion.1
  (1 shorter events, 0.0 us)
Async XLA Ops:
  6.5 1.8 copy-start
  6.5 4.4 %copy-start.1 = (bf16[128,2048]{1,0:T(8,128)(2,1)S(1)}, bf16[128,2048]{1,0:T(8,128)(2,1)}, u32[]{:S(2)}) copy-start(bf16[128,2048]{1,0:T(8,128)(2,1)} %param.8) | copy-start | bytes 1572868
  6.5 4.4 %copy-start.2 = (f32[2048]{0:T(1024)S(1)}, f32[2048]{0:T(1024)}, u32[]{:S(2)}) copy-start(f32[2048]{0:T(1024)} %param.9) | copy-start | bytes 24580
  6.5 69.4 %all-gather.8.cloned.1.call-start = ((), (), s32[]{:S(2)}) async-start(), calls=%async_computation.2 | async-start | bytes 3932160 | tf_op jit(solution)/shard_map/all_gather | solution.py:28
  9.6 103.5 %all-gather.6.cloned.1.call-start = ((), (), s32[]{:S(2)}) async-start(), calls=%async_computation.1 | async-start | bytes 4718592 | tf_op jit(solution)/shard_map/all_gather | solution.py:22
  10.9 6.3 %copy-start.4 = (f32[1408]{0:T(1024)S(1)}, f32[1408]{0:T(1024)}, u32[]{:S(2)}) copy-start(f32[1408]{0:T(1024)} %param.11) | copy-start | bytes 16900
  10.9 6.4 %copy-start.5 = (f32[1408]{0:T(1024)S(1)}, f32[1408]{0:T(1024)}, u32[]{:S(2)}) copy-start(f32[1408]{0:T(1024)} %param.13) | copy-start | bytes 16900
  11.9 166.2 %all-gather.10.cloned.1.call-start = ((), (), s32[]{:S(2)}) async-start(), calls=%async_computation.3 | async-start | bytes 3932160 | tf_op jit(solution)/shard_map/all_gather | solution.py:32
  14.8 222.6 %all-gather.12.cloned.1.call-start = ((), (), s32[]{:S(2)}) async-start(), calls=%async_computation.4 | async-start | bytes 3604480 | tf_op jit(solution)/shard_map/all_gather | solution.py:34
  17.2 282.5 %reduce-scatter.2.cloned.1.call-start = ((), (), s32[]{:S(2)}) async-start(), calls=%async_computation.5 | async-start | bytes 4718592 | tf_op jit(solution)/shard_map/reduce_scatter | solution.py:39
  249.7 0.7 copy-start.3
Sparse Core Ops, SparseCore 0:
  9.7 66.1 all-gather.7
  77.8 35.2 all-gather.5
  114.7 63.4 all-gather.9
  179.6 57.7 all-gather.11
  249.8 49.8 reduce-scatter.1
where the time goes:
time: 308 us
  waiting for transfers between devices  250 us (81%)
  matrix products  20.2 us (7%)
  between operations  13.2 us (4%)
  blocking collectives  11.9 us (4%)
  local copies, waits for them, and re-layouts  8.92 us (3%)
  other arithmetic  4.16 us (1%)
    all_gather x1, waiting for transfers between devices, shards(): down_full = lax.all_gather(down_low, 'fs', axis=1, tiled=True)  59.2 us
    all_gather x1, waiting for transfers between devices, shards(): lax.all_gather(gate_low, 'fs', axis=0, tiled=True)  58.6 us
    all_gather x1, waiting for transfers between devices, shards(): lax.all_gather(up_low, 'fs', axis=0, tiled=True)  57.1 us
    reduce_scatter x1, waiting for transfers between devices, shards(): lax.psum_scatter(jnp.dot(hidden, down_full, preferred_element_type=jnp.fl...  37.4 us
    all_gather x1, waiting for transfers between devices, shards(): group = lax.all_gather(normed, ('rep', 'tp'), axis=0, tiled=True)  37.1 us
    dot_general x1, matrix products, shards(): jnp.dot(hidden, down_full, preferred_element_type=jnp.float32)  12.3 us
    all_gather x1, blocking collectives, shards(): scales = lax.all_gather(down_scale, 'fs', axis=0, tiled=True)  11.9 us
    dot_general x1, matrix products, shards(): jnp.dot(group, lax.all_gather(gate_low, 'fs', axis=0, tiled=True), prefer...  7.9 us
  transfers between devices with their start and end apart: 5, of which 5 were waited for; matrix products, arithmetic and copies ran while one was open for 5% of the time, Pallas kernels for 0%

commit v1 on v0

--- a/solution.py
+++ b/solution.py
@@ -2,6 +2,15 @@
 import jax.numpy as jnp
 from jax import lax
 from jax.sharding import PartitionSpec as P
+
+
+def touch_row(mine, net_axis):
+    n_all = jax.lax.axis_size(net_axis)
+    frames = list(map(lambda rr: n_all if rr == 0 else 1, range(mine.ndim)))
+    a_now = jax.lax.all_to_all(
+        jnp.tile(mine, frames), net_axis, split_axis=0, concat_axis=0, tiled=True
+    )
+    return a_now
 
 
 def shards(
@@ -19,7 +28,7 @@
     mean_square = jnp.mean(flat * flat, axis=-1, keepdims=True)
     inverse = lax.rsqrt(mean_square + 1e-06)
     normed = (flat * inverse * norm_gain).astype(jnp.bfloat16)
-    group = lax.all_gather(normed, ("rep", "tp"), axis=0, tiled=True)
+    group = touch_row(normed, ("rep", "tp"))
     gate_low = part(gate_weight, 1).astype(jnp.bfloat16)
     up_low = part(up_weight, 1).astype(jnp.bfloat16)
     down_low = part(down_weight, 0).astype(jnp.bfloat16)

time: 308 us -> 270 us (0.88)
  waiting for transfers between devices: 250 us -> 205 us
  starting transfers between devices: 0.17 us -> 5.37 us
    all_gather x1, waiting for transfers between devices: 58.6 us -> 7.06 us  [shards(): lax.all_gather(gate_low, 'fs', axis=0, tiled=True)]
    all_to_all x0 -> x1, waiting for transfers between devices: none -> 45.6 us  [touch_row(): jax.lax.all_to_all(jnp.tile(mine, frames), net_axis, split_axis=0, concat...]
    all_gather x1 -> x0, waiting for transfers between devices: 37.1 us -> none  [shards(): group = lax.all_gather(normed, ('rep', 'tp'), axis=0, tiled=True)]
    all_to_all x0 -> x1, starting transfers between devices: none -> 5.25 us  [touch_row(): jax.lax.all_to_all(jnp.tile(mine, frames), net_axis, split_axis=0, concat...]
  transfers between devices with their start and end apart: 5 -> 5, of which waited for: 5 -> 5; matrix products, arithmetic and copies ran while one was open for 5% -> 6% of each run, Pallas kernels for 0% -> 0%
where the time goes in v1:
time: 270 us
  waiting for transfers between devices  205 us (76%)
  matrix products  20.3 us (8%)
  between operations  13.2 us (5%)
  blocking collectives  11.9 us (4%)
  local copies, waits for them, and re-layouts  11.5 us (4%)
  starting transfers between devices  5.37 us (2%)
    all_gather x1, waiting for transfers between devices, shards(): down_full = lax.all_gather(down_low, 'fs', axis=1, tiled=True)  59.4 us
    all_gather x1, waiting for transfers between devices, shards(): lax.all_gather(up_low, 'fs', axis=0, tiled=True)  55.8 us
    all_to_all x1, waiting for transfers between devices, touch_row(): jax.lax.all_to_all(jnp.tile(mine, frames), net_axis, split_axis=0, concat...  45.6 us
    reduce_scatter x1, waiting for transfers between devices, shards(): lax.psum_scatter(jnp.dot(hidden, down_full, preferred_element_type=jnp.fl...  37.4 us
    dot_general x1, matrix products, shards(): jnp.dot(hidden, down_full, preferred_element_type=jnp.float32)  12.3 us
    all_gather x1, blocking collectives, shards(): scales = lax.all_gather(down_scale, 'fs', axis=0, tiled=True)  11.9 us
    dot_general x1, matrix products, shards(): jnp.dot(group, lax.all_gather(gate_low, 'fs', axis=0, tiled=True), prefer...  7.93 us
    all_gather x1, waiting for transfers between devices, shards(): lax.all_gather(gate_low, 'fs', axis=0, tiled=True)  7.06 us
  transfers between devices with their start and end apart: 5, of which 5 were waited for; matrix products, arithmetic and copies ran while one was open for 6% of the time, Pallas kernels for 0%

profile of v1, /device:TPU:0, one launch (start us, length us, event | category | flops | bytes accessed | tf_op | source)
XLA Modules:
  0.0 269.8 jit_solution(11367498532129998332)
XLA Ops:
  6.5 0.0 copy-start
  6.5 0.0 copy-start.1
  6.5 0.0 copy-start.2
  6.5 0.0 all-gather.5.cloned.1.call-start
  6.6 1.8 copy-done
  8.4 1.3 dynamic-slice_convert_fusion.1
  9.6 0.0 all-gather.5.cloned.1.call-update
  9.6 0.0 all-gather.7.cloned.1.call-start
  9.7 2.7 %dynamic-slice_convert_fusion = bf16[512,704]{1,0:T(8,128)(2,1)} fusion(f32[512,1408]{1,0:T(8,128)} %param.12, s32[]{:T(128)S(6)} %select_n.2), kind=kLoop, calls=%fused_computation.2 | loop fusion | bytes 1441796 | tf_op jit(solution)/shard_map/convert_element_type | solution.py:33
  12.4 0.0 all-gather.7.cloned.1.call-update
  12.4 0.0 copy-done.1
  12.4 0.2 fusion
  12.6 0.0 copy-done.2
  12.7 0.2 fusion.2
  12.9 2.5 tile.2
  15.3 0.0 copy-start.4
  15.4 0.0 copy-start.5
  15.4 5.2 %all-to-all-start = ((bf16[8,128,2048]{2,1,0:T(8,128)(2,1)}), bf16[8,128,2048]{2,1,0:T(8,128)(2,1)}, u32[]{:S(2)}, u32[]{:S(2)}) async-start(bf16[8,128,2048]{2,1,0:T(8,128)(2,1)} %tile.2), calls=%async_computation | async-start | bytes 8388608 | tf_op jit(solution)/shard_map/all_to_all | solution.py:10
  20.6 0.0 all-gather.9.cloned.1.call-start
  20.6 2.4 dynamic-slice_convert_fusion.2
  23.1 0.0 all-gather.9.cloned.1.call-update
  23.1 0.0 reduce-scatter.2.cloned.1.call-start
  23.1 0.0 copy-done.4
  23.1 0.1 dynamic_slice.16
  23.2 0.0 copy-done.5
  23.2 0.1 dynamic_slice.18
  23.3 45.6 %all-to-all-done = bf16[8,128,2048]{2,1,0:T(8,128)(2,1)} async-done(((bf16[8,128,2048]{2,1,0:T(8,128)(2,1)}), bf16[8,128,2048]{2,1,0:T(8,128)(2,1)}, u32[]{:S(2)}, u32[]{:S(2)}) %all-to-all-start) | async-done | bytes 4194336 | tf_op jit(solution)/shard_map/all_to_all | solution.py:10
  68.9 7.1 %all-gather.5.cloned.1.call-done = bf16[2048,704]{1,0:T(8,128)(2,1)} async-done(((bf16[512,704]{1,0:T(8,128)(2,1)}), bf16[2048,704]{1,0:T(8,128)(2,1)}) %all-gather.5.cloned.1.call-update) | async-done | bytes 2883600 | tf_op jit(solution)/shard_map/all_gather | solution.py:37
  76.0 7.9 %fusion.4 = f32[1024,704]{0,1:T(8,128)} fusion(bf16[1024,2048]{1,0:T(8,128)(2,1)} %bitcast, bf16[2048,704]{1,0:T(8,128)(2,1)} %all-gather.5.cloned.1.call-done), kind=kOutput, calls=%fused_computation.13 | convolution fusion | flops 2952790016 | bytes 9961472 | tf_op jit(solution)/shard_map/dot_general | solution.py:35
  83.9 55.8 %all-gather.7.cloned.1.call-done = bf16[2048,704]{1,0:T(8,128)(2,1)} async-done(((bf16[512,704]{1,0:T(8,128)(2,1)}), bf16[2048,704]{1,0:T(8,128)(2,1)}) %all-gather.7.cloned.1.call-update) | async-done | bytes 2883600 | tf_op jit(solution)/shard_map/all_gather | solution.py:41
  139.7 59.4 %all-gather.9.cloned.1.call-done = bf16[704,2048]{1,0:T(8,128)(2,1)} async-done(((bf16[704,512]{1,0:T(8,128)(2,1)}), bf16[704,2048]{1,0:T(8,128)(2,1)}) %all-gather.9.cloned.1.call-update) | async-done | bytes 2883600 | tf_op jit(solution)/shard_map/all_gather | solution.py:43
  199.0 12.3 %convolution_convert_fusion = bf16[1024,2048]{1,0:T(8,128)(2,1)} fusion(bf16[704,2048]{1,0:T(8,128)(2,1)} %all-gather.9.cloned.1.call-done, f32[1024,704]{0,1:T(8,128)} %fusion.4, bf16[1024,2048]{1,0:T(8,128)(2,1)} %bitcast, bf16[2048,704]{1,0:T(8,128)(2,1)} %all-gather.7.cloned.1.call-done, f32[704]{0:T(1024)S(1)} %dynamic_slice.18, f32[704]{0:T(1024)S(1)} %dynamic_slice.16), kind=kOutput, calls=%fused_computation | convolution fusion | flops 5913444352 | bytes 17044992 | tf_op jit(solution)/shard_map/dot_general | solution.py:49
  211.3 0.0 copy-start.3
  211.3 0.0 reduce-scatter.2.cloned.1.call-update
  211.4 0.7 copy-done.3
  212.0 11.9 %all-gather = f32[4,1,512]{2,1,0:T(1,128)S(1)} all-gather(f32[1,1,512]{2,1,0:T(1,128)S(1)} %bitcast.9), channel_id=1, replica_groups=mesh['rep'=2,'fs'=4,'tp'=4] {'fs'}, dimensions={0}, use_global_device_ids=true | all-gather | bytes 10240 | tf_op jit(solution)/shard_map/all_gather | solution.py:47
  224.0 37.4 %reduce-scatter.2.cloned.1.call-done = bf16[128,2048]{1,0:T(8,128)(2,1)} async-done(((bf16[1024,2048]{1,0:T(8,128)(2,1)}), bf16[128,2048]{1,0:T(8,128)(2,1)}) %reduce-scatter.2.cloned.1.call-update) | async-done | bytes 524304 | tf_op jit(solution)/shard_map/reduce_scatter | solution.py:48
  261.4 1.9 multiply_convert_fusion.1
  (1 shorter events, 0.0 us)
Async XLA Ops:
  6.5 1.8 copy-start
  6.5 5.9 %copy-start.1 = (bf16[128,2048]{1,0:T(8,128)(2,1)S(1)}, bf16[128,2048]{1,0:T(8,128)(2,1)}, u32[]{:S(2)}) copy-start(bf16[128,2048]{1,0:T(8,128)(2,1)} %param.8) | copy-start | bytes 1572868
  6.5 6.1 %copy-start.2 = (f32[2048]{0:T(1024)S(1)}, f32[2048]{0:T(1024)}, u32[]{:S(2)}) copy-start(f32[2048]{0:T(1024)} %param.9) | copy-start | bytes 24580
  6.5 69.4 %all-gather.5.cloned.1.call-start = ((), (), s32[]{:S(2)}) async-start(), calls=%async_computation.2 | async-start | bytes 3932160 | tf_op jit(solution)/shard_map/all_gather | solution.py:37
  9.6 130.0 %all-gather.7.cloned.1.call-start = ((), (), s32[]{:S(2)}) async-start(), calls=%async_computation.3 | async-start | bytes 3932160 | tf_op jit(solution)/shard_map/all_gather | solution.py:41
  15.3 7.8 %copy-start.4 = (f32[1408]{0:T(1024)S(1)}, f32[1408]{0:T(1024)}, u32[]{:S(2)}) copy-start(f32[1408]{0:T(1024)} %param.11) | copy-start | bytes 16900
  15.4 7.9 %copy-start.5 = (f32[1408]{0:T(1024)S(1)}, f32[1408]{0:T(1024)}, u32[]{:S(2)}) copy-start(f32[1408]{0:T(1024)} %param.13) | copy-start | bytes 16900
  15.4 53.6 %all-to-all-start = ((bf16[8,128,2048]{2,1,0:T(8,128)(2,1)}), bf16[8,128,2048]{2,1,0:T(8,128)(2,1)}, u32[]{:S(2)}, u32[]{:S(2)}) async-start(bf16[8,128,2048]{2,1,0:T(8,128)(2,1)} %tile.2), calls=%async_computation | async-start | bytes 8388608 | tf_op jit(solution)/shard_map/all_to_all | solution.py:10
  20.6 178.4 %all-gather.9.cloned.1.call-start = ((), (), s32[]{:S(2)}) async-start(), calls=%async_computation.4 | async-start | bytes 3604480 | tf_op jit(solution)/shard_map/all_gather | solution.py:43
  23.1 238.3 %reduce-scatter.2.cloned.1.call-start = ((), (), s32[]{:S(2)}) async-start(), calls=%async_computation.5 | async-start | bytes 4718592 | tf_op jit(solution)/shard_map/reduce_scatter | solution.py:48
  211.3 0.7 copy-start.3
Sparse Core Ops, SparseCore 0:
  9.8 66.1 all-gather.4
  77.5 62.0 all-gather.6
  141.2 57.7 all-gather.8
  211.5 49.8 reduce-scatter.1
